TPU v7x, 512 devices: a whole 4x4x16 slice. The times are simulated.
512 devices in a mesh: sp: 32 (over z, core), tp: 16 (over y, x).
Axes of the slice: x: 4, y: 4, z: 16, core: 2. Of those that a mesh axis runs over, the one named last changes fastest.
Arguments:
- queries: bfloat16 [8192, 2048], P('sp', 'tp'), may hold values from -6 to 6
- keys: bfloat16 [8192, 256], P('sp'), may hold values from -6 to 6
- values: bfloat16 [8192, 256], P('sp'), may hold values from -6 to 6
- query_gain: float32 [128], replicated, may hold values from 0.1 to 5.5
- key_gain: float32 [128], replicated, may hold values from 0.1 to 5.5
- out_proj: bfloat16 [2048, 2048], P(None, 'tp'), may hold values from -0.125 to 0.125
- expert_norm_scale: float32 [2048], replicated, may hold values from 0.1 to 1.9
- residual: bfloat16 [8192, 2048], P(('sp', 'tp')), may hold values from -6 to 6
- routes: int32 [8192, 2], P(('sp', 'tp')), may hold values from 0 to 31, all different within a row; in each aligned block of 16 rows (0 to 15, 16 to 31, ...) at most 2 rows name the same one
- route_weights: float32 [8192, 2], P(('sp', 'tp')), may hold values from 0.1 to 0.9
- w_gate: bfloat16 [32, 2048, 4096], P('sp', None, 'tp'), may hold values from -0.125 to 0.125
- w_up: bfloat16 [32, 2048, 4096], P('sp', None, 'tp'), may hold values from -0.125 to 0.125
- w_down: bfloat16 [32, 4096, 2048], P('sp', 'tp'), may hold values from -0.09375 to 0.09375
Outputs:
- layer_out: bfloat16 [8192, 2048], P(('sp', 'tp'))
Inputs may be any that keep to these rules, and one draw needn't show every extreme that they name: `routes`: in the rows of one device no expert is named by more than 2 rows, a bound that some block reaches; a row names 2 different experts.
All inputs are finite; a program needn't handle non-finite values.
Results may differ from a plain program's by a relative error of at most 0.0095.
The roundings to bfloat16 on the way count: a program that leaves them out, or rounds other values in their place, can miss the bound.
Values may be sent and summed in bfloat16 or wider, within the bound.
No kernel may reach another device: no remote copies, remote signals or barrier semaphores. Data moves between devices by JAX's collectives and lax.ppermute only.
A program may use at most 64 MiB of HBM per device.

v0:
```python
import jax
import jax.numpy as jnp
from jax import lax
from jax.sharding import PartitionSpec as P

GRID_W = 64
EPS = 1e-06
ROPE_BASE = 10000.0
NEG_START = -1e30


def side_by_side(arrays, axis, dim, along):
    both = jnp.concatenate(arrays, axis=along)
    result, at, done = (lax.all_gather(both, axis, axis=dim, tiled=True), 0, [])
    for a in arrays:
        done.append(lax.slice_in_dim(result, at, at + a.shape[along], axis=along))
        at += a.shape[along]
    return tuple(done)


def joined_along(tiles, dim):
    dims = list(tiles.shape[1:])
    dims[dim] *= tiles.shape[0]
    return jnp.moveaxis(tiles, 0, dim).reshape(dims)


def copy_for_each(value, axis):
    copies = jnp.broadcast_to(value, (lax.axis_size(axis), *value.shape))
    return lax.all_to_all(copies, axis, split_axis=0, concat_axis=0, tiled=True)


def gather_directly(value, axis, dim):
    return joined_along(copy_for_each(value, axis), dim)


def split_up(value, dim, peers):
    before, after = (value.shape[:dim], value.shape[dim + 1 :])
    return jnp.moveaxis(value.reshape(*before, peers, -1, *after), dim, 0)


def sent_and_summed(value, axis, dim):
    peers = lax.axis_size(axis)
    tiles = lax.all_to_all(split_up(value, dim, peers), axis, 0, 0, tiled=True)
    return jnp.sum(tiles.astype(jnp.float32), axis=0)


def rotate(field, position):
    half = field.shape[-1] // 2
    quarter = half // 2
    freqs = ROPE_BASE ** (-jnp.arange(quarter, dtype=jnp.float32) / quarter)
    grid_row = (position // GRID_W).astype(jnp.float32)
    grid_col = (position % GRID_W).astype(jnp.float32)

    def turn_half(part, coord):
        angle = coord[:, None] * freqs[None, :]
        cosine = jnp.cos(angle)[:, None, :]
        sine = jnp.sin(angle)[:, None, :]
        first, second = (part[..., :quarter], part[..., quarter:])
        return jnp.concatenate(
            [first * cosine - second * sine, second * cosine + first * sine], axis=-1
        )

    return jnp.concatenate(
        [turn_half(field[..., :half], grid_row), turn_half(field[..., half:], grid_col)], axis=-1
    )


def prepare(field, gain, position):
    count = field.shape[0]
    width = gain.shape[0]
    heads_here = field.shape[1] // width
    values_f = field.reshape(count, heads_here, width).astype(jnp.float32)
    scaled = (
        values_f * lax.rsqrt(jnp.mean(values_f * values_f, axis=-1, keepdims=True) + EPS) * gain
    )
    return rotate(scaled, position).reshape(count, heads_here * width).astype(jnp.bfloat16)


def absorb(carry, query_matrix, key_rows, value_rows, scale):
    count = key_rows.shape[0]
    width = 2048
    key_blocks = key_rows.reshape(count // width, width, key_rows.shape[1], key_rows.shape[2])
    value_blocks = value_rows.reshape(
        count // width, width, value_rows.shape[1], value_rows.shape[2]
    )

    def step(state, block):
        run_max, run_sum, run_acc = state
        key_tile_rows, value_tile_rows = block
        scores = (
            jnp.einsum(
                "hxt,ght->hxg", query_matrix, key_tile_rows, preferred_element_type=jnp.float32
            )
            * scale
        )
        new_max = jnp.maximum(run_max, jnp.max(scores, axis=-1))
        weight_tensors = jnp.exp(scores - new_max[..., None]).astype(jnp.bfloat16)
        factor = jnp.exp(run_max - new_max)
        run_sum = run_sum * factor + jnp.sum(weight_tensors.astype(jnp.float32), axis=-1)
        run_acc = run_acc * factor[..., None] + jnp.einsum(
            "zij,jzu->ziu", weight_tensors, value_tile_rows, preferred_element_type=jnp.float32
        )
        return ((new_max, run_sum, run_acc), None)

    result, unused = lax.scan(step, carry, (key_blocks, value_blocks))
    return result


def start_state(batch, rows, width):
    return (
        jnp.full((batch, rows), NEG_START, jnp.float32),
        jnp.zeros((batch, rows), jnp.float32),
        jnp.zeros((batch, rows, width), jnp.float32),
    )


def local(
    queries,
    keys,
    values,
    query_gain,
    key_gain,
    out_proj,
    expert_norm_scale,
    residual,
    routes,
    route_weights,
    w_gate,
    w_up,
    w_down,
):
    head_size = query_gain.shape[0]
    tok_sp = queries.shape[0]
    tp_count = lax.axis_size("tp")
    sp_count = lax.axis_size("sp")
    heads_dev = queries.shape[1] // head_size
    all_heads = heads_dev * tp_count
    kv_heads = keys.shape[1] // head_size
    group = all_heads // kv_heads
    scale = head_size ** (-0.5)
    tp_index = lax.axis_index("tp")
    sp_index = lax.axis_index("sp")
    position = sp_index * tok_sp + jnp.arange(tok_sp, dtype=jnp.int32)
    q_rot = prepare(queries, query_gain, position)
    shared_value_head = tp_index * heads_dev // group
    own_keys = prepare(
        lax.dynamic_slice_in_dim(keys, shared_value_head * head_size, head_size, 1),
        key_gain,
        position,
    )
    own_values = lax.dynamic_slice_in_dim(values, shared_value_head * head_size, head_size, 1)
    query_matrix = q_rot.reshape(tok_sp, heads_dev, head_size).transpose(1, 0, 2)
    key_piece, value_piece = side_by_side((own_keys, own_values), "sp", 0, 1)
    run_max, run_sum, run_acc = absorb(
        start_state(1, heads_dev * tok_sp, head_size),
        query_matrix,
        key_piece[:, None, :],
        value_piece[:, None, :],
        scale,
    )
    attn = (run_acc / run_sum[..., None]).astype(jnp.bfloat16)
    attn = attn.transpose(1, 0, 2).reshape(tok_sp, heads_dev * head_size)
    columns = jnp.dot(gather_directly(attn, "tp", 1), out_proj, preferred_element_type=jnp.float32)
    projected = lax.all_to_all(
        columns.astype(jnp.bfloat16), "tp", split_axis=0, concat_axis=1, tiled=True
    )
    mixed_float_output = residual.astype(jnp.float32) + projected.astype(jnp.float32)
    mixed = mixed_float_output.astype(jnp.bfloat16)
    mixed_float_output = mixed.astype(jnp.float32)
    normed = (
        mixed_float_output
        * lax.rsqrt(jnp.mean(mixed_float_output * mixed_float_output, axis=-1, keepdims=True) + EPS)
        * expert_norm_scale
    ).astype(jnp.bfloat16)
    tok_dev = residual.shape[0]
    top = routes.shape[1]
    capacity = max(2, 2 * tok_dev * top // sp_count)
    flat_routes = routes.reshape(-1)
    one_hot = (flat_routes[:, None] == jnp.arange(sp_count, dtype=jnp.int32)[None, :]).astype(
        jnp.int32
    )
    earlier = jnp.cumsum(one_hot, axis=0) - one_hot
    slot_index = jnp.sum(earlier * one_hot, axis=1)
    target = flat_routes * capacity + slot_index
    selector = (
        jnp.arange(sp_count * capacity, dtype=jnp.int32)[:, None] == target[None, :]
    ).astype(jnp.bfloat16)
    selector = jnp.sum(selector.reshape(sp_count * capacity, tok_dev, top), axis=2)
    send_rows = jnp.dot(selector, normed, preferred_element_type=jnp.float32).astype(jnp.bfloat16)
    arrived = lax.all_to_all(send_rows, "sp", split_axis=0, concat_axis=0, tiled=True)
    gate_weight = w_gate[0]
    up_weight = w_up[0]
    down_weight = w_down[0]
    piece = lax.all_gather(arrived, "tp", axis=0, tiled=True)
    gate = jnp.dot(piece, gate_weight, preferred_element_type=jnp.float32)
    upper = jnp.dot(piece, up_weight, preferred_element_type=jnp.float32)
    hidden = (jax.nn.silu(gate) * upper).astype(jnp.bfloat16)
    expert_out = sent_and_summed(
        jnp.dot(hidden, down_weight, preferred_element_type=jnp.float32).astype(jnp.bfloat16),
        "tp",
        0,
    ).astype(jnp.bfloat16)
    returned = lax.all_to_all(expert_out, "sp", split_axis=0, concat_axis=0, tiled=True)
    picked = (
        jnp.take(returned, target, axis=0)
        .astype(jnp.float32)
        .reshape(tok_dev, top, returned.shape[1])
    )
    moe_sum = jnp.sum(picked * route_weights[:, :, None], axis=1)
    return (mixed_float_output + moe_sum).astype(jnp.bfloat16)


def solution(mesh):
    placed = (
        P("sp", "tp"),
        P("sp", None),
        P("sp", None),
        P(),
        P(),
        P(None, "tp"),
        P(),
        P(("sp", "tp"), None),
        P(("sp", "tp"), None),
        P(("sp", "tp"), None),
        P("sp", None, "tp"),
        P("sp", None, "tp"),
        P("sp", "tp", None),
    )
    return jax.shard_map(
        local, mesh=mesh, in_specs=placed, out_specs=P(("sp", "tp"), None), check_vma=False
    )
```

profile of v0, /device:TPU:1, one launch (start us, length us, event | category | flops | bytes accessed | tf_op | source)
XLA Modules:
  0.0 363.4 jit_solution(8110786324239800701)
XLA Ops:
  6.6 1.0 constant_dynamic-slice_fusion
  7.5 0.1 copy.48
  7.7 0.9 copy.36
  8.8 0.7 fusion.25
  9.6 0.7 fusion.28
  10.3 0.3 fusion.55
  10.7 0.7 pad_maximum_fusion
  11.4 0.1 copy.39
  11.5 86.4 %all-gather.3.cloned.1.call-done = bf16[8192,256]{0,1:T(8,128)(2,1)} async-done(((bf16[256,256]{0,1:T(8,128)(2,1)}), bf16[8192,256]{0,1:T(8,128)(2,1)}) %all-gather.3.cloned.1.call-update) | async-done | bytes 4194320 | tf_op jit(solution)/shard_map/all_gather | solution.py:14
  97.9 3.9 %fusion.82 = (bf16[8192,128]{0,1:T(8,128)(2,1)S(1)}, bf16[8192,128]{0,1:T(8,128)(2,1)}) fusion(bf16[8192,256]{0,1:T(8,128)(2,1)} %all-gather.3.cloned.1.call-done), kind=kLoop, calls=%fused_computation.132 | loop fusion | bytes 8388608 | tf_op jit(solution)/shard_map/slice | solution.py:16
  101.8 4.1 %copy.35 = bf16[8192,128]{1,0:T(8,128)(2,1)} copy(bf16[8192,128]{0,1:T(8,128)(2,1)} %get-tuple-element.113) | data formatting | bytes 4194304 | tf_op jit(solution)/shard_map/slice | solution.py:16
  105.9 2.4 copy.37
  108.4 14.2 %while.15 = (s32[]{:T(128)}, f32[1,256]{1,0:T(1,128)S(1)}, f32[1,256]{1,0:T(1,128)S(1)}, f32[1,256,128]{2,1,0:T(8,128)S(1)}, bf16[4,2048,1,128]{3,1,2,0:T(8,128)...) while((s32[]{:T(128)}, f32[1,256]{1,0:T(1,128)S(1)}, ...), condition=%wide.region_5.6_spmd.clone, body=%wide.region_2.5_spmd.clone.sunk | while | flops 272729344 | bytes 7685225 | solution.py:105
  108.4 1.5 fusion.94
  110.0 0.4 convert_reduce_fusion.2
  110.3 1.6 fusion.97
  111.9 1.6 fusion.94
  113.5 0.4 convert_reduce_fusion.2
  113.9 1.6 fusion.97
  115.5 1.6 fusion.94
  117.1 0.4 convert_reduce_fusion.2
  117.4 1.6 fusion.97
  119.0 1.6 fusion.94
  120.6 0.4 convert_reduce_fusion.2
  121.0 1.6 fusion.97
  122.8 1.1 broadcast_in_dim.18
  123.9 6.7 %all-to-all-start = ((bf16[16,256,128]{1,2,0:T(8,128)(2,1)}), bf16[16,256,128]{1,2,0:T(8,128)(2,1)S(1)}, u32[]{:S(2)}, u32[]{:S(2)}) async-start(bf16[16,256,128]{1,2,0:T(8,128)(2,1)} %broadcast_in_dim.18), calls=%async_computation | async-start | bytes 2097152 | tf_op jit(solution)/shard_map/all_to_all | solution.py:29
  130.9 0.2 select_reduce_fusion
  131.3 15.7 %all-to-all-done = bf16[16,256,128]{1,2,0:T(8,128)(2,1)S(1)} async-done(((bf16[16,256,128]{1,2,0:T(8,128)(2,1)}), bf16[16,256,128]{1,2,0:T(8,128)(2,1)S(1)}, u32[]{:S(2)}, u32[]{:S(2)}) %all-to-all-start) | async-done | bytes 1048608 | tf_op jit(solution)/shard_map/all_to_all | solution.py:29
  147.0 1.1 convolution_convert_fusion.2
  148.1 4.5 %all-to-all-start.1 = ((bf16[16,16,128]{2,1,0:T(8,128)(2,1)}), bf16[16,16,128]{2,1,0:T(8,128)(2,1)S(1)}, u32[]{:S(2)}, u32[]{:S(2)}) async-start(bf16[16,16,128]{2,1,0:T(8,128)(2,1)} %bitcast.12), calls=%async_computation.1 | async-start | bytes 131072 | tf_op jit(solution)/shard_map/all_to_all | solution.py:164
  152.8 6.4 %all-to-all-done.1 = bf16[16,16,128]{2,1,0:T(8,128)(2,1)S(1)} async-done(((bf16[16,16,128]{2,1,0:T(8,128)(2,1)}), bf16[16,16,128]{2,1,0:T(8,128)(2,1)S(1)}, u32[]{:S(2)}, u32[]{:S(2)}) %all-to-all-start.1) | async-done | bytes 65568 | tf_op jit(solution)/shard_map/all_to_all | solution.py:164
  159.2 0.1 fusion.29
  159.3 0.3 convolution_convert_fusion.1
  159.6 0.2 all_to_all.35
  159.8 30.5 %all_to_all.47 = bf16[32,2,2048]{2,1,0:T(2,128)(2,1)S(1)} all-to-all(bf16[32,2,2048]{2,1,0:T(2,128)(2,1)S(1)} %all_to_all.35), channel_id=1, replica_groups=mesh['sp'=32,'tp'=16] {'sp'}, dimensions={0} | all-to-all | bytes 524288 | tf_op jit(solution)/shard_map/all_to_all | solution.py:190
  190.3 0.8 all_to_all.37
  191.1 54.4 %all-gather.5.cloned.1.call-done = bf16[1024,2048]{1,0:T(8,128)(2,1)} async-done(((bf16[64,2048]{1,0:T(8,128)(2,1)}), bf16[1024,2048]{1,0:T(8,128)(2,1)}) %all-gather.5.cloned.1.call-update) | async-done | bytes 4194320 | tf_op jit(solution)/shard_map/all_gather | solution.py:194
  245.5 4.5 %fusion.15 = f32[1024,256]{1,0:T(8,128)} fusion(bf16[1024,2048]{1,0:T(8,128)(2,1)} %all-gather.5.cloned.1.call-done, bf16[1,2048,256]{2,1,0:T(8,128)(2,1)S(1)} %copy-done.6), kind=kOutput, calls=%fused_computation.27 | convolution fusion | flops 1073741824 | bytes 6291456 | tf_op jit(solution)/shard_map/dot_general | solution.py:195
  250.0 9.1 %convolution_convert_fusion = bf16[1024,2048]{1,0:T(8,128)(2,1)} fusion(bf16[1024,2048]{1,0:T(8,128)(2,1)} %all-gather.5.cloned.1.call-done, bf16[1,256,2048]{2,1,0:T(8,128)(2,1)S(1)} %copy-done, bf16[1,2048,256]{2,1,0:T(8,128)(2,1)} %param.26, f32[1024,256]{1,0:T(8,128)} %fusion.15), kind=kOutput, calls=%fused_computation.20 | convolution fusion | flops 2151153664 | bytes 11534336 | tf_op jit(solution)/shard_map/dot_general | solution.py:199
  259.1 55.0 %all_to_all.48 = bf16[16,64,2048]{2,1,0:T(8,128)(2,1)} all-to-all(bf16[16,64,2048]{2,1,0:T(8,128)(2,1)} %bitcast.91), channel_id=1, replica_groups=mesh['sp'=32,'tp'=16] {'tp'}, dimensions={0} | all-to-all | bytes 8388608 | tf_op jit(solution)/shard_map/all_to_all | solution.py:43
  314.1 3.0 reduce_sum.90
  317.1 0.9 all_to_all.39
  317.9 14.3 %all-to-all-start.4 = ((bf16[32,2,2048]{2,1,0:T(2,128)(2,1)}), bf16[32,2,2048]{2,1,0:T(2,128)(2,1)S(1)}, u32[]{:S(2)}, u32[]{:S(2)}) async-start(bf16[32,2,2048]{2,1,0:T(2,128)(2,1)} %all_to_all.39), calls=%async_computation.4 | async-start | bytes 524288 | tf_op jit(solution)/shard_map/all_to_all | solution.py:203
  332.6 21.9 %all-to-all-done.4 = bf16[32,2,2048]{2,1,0:T(2,128)(2,1)S(1)} async-done(((bf16[32,2,2048]{2,1,0:T(2,128)(2,1)}), bf16[32,2,2048]{2,1,0:T(2,128)(2,1)S(1)}, u32[]{:S(2)}, u32[]{:S(2)}) %all-to-all-start.4) | async-done | bytes 262176 | tf_op jit(solution)/shard_map/all_to_all | solution.py:203
  354.6 0.7 gather_fusion
  355.3 0.6 multiply_reduce_fusion
  355.9 0.6 fusion.32
  (62 shorter events, 1.8 us)
Async XLA Ops:
  6.5 243.5 %copy-start = (bf16[1,256,2048]{2,1,0:T(8,128)(2,1)S(1)}, bf16[1,256,2048]{2,1,0:T(8,128)(2,1)}, u32[]{:S(2)}) copy-start(bf16[1,256,2048]{2,1,0:T(8,128)(2,1)} %param.27) | copy-start | bytes 3145732
  6.5 91.4 %all-gather.3.cloned.1.call-start = ((), (), s32[]{:S(2)}) async-start(), calls=%async_computation.5 | async-start | bytes 4325376 | tf_op jit(solution)/shard_map/all_gather | solution.py:14
  122.6 8.0 %copy-start.3 = (s32[16,2]{0,1:T(2,128)S(1)}, s32[16,2]{0,1:T(2,128)}, u32[]{:S(2)}) copy-start(s32[16,2]{0,1:T(2,128)} %param.23) | copy-start | bytes 388
  122.6 24.4 %copy-start.1 = (bf16[2048,128]{1,0:T(8,128)(2,1)S(1)}, bf16[2048,128]{1,0:T(8,128)(2,1)}, u32[]{:S(2)}) copy-start(bf16[2048,128]{1,0:T(8,128)(2,1)} %param.20) | copy-start | bytes 1572868
  123.9 35.2 %copy-start.2 = (bf16[16,2048]{1,0:T(8,128)(2,1)S(1)}, bf16[16,2048]{1,0:T(8,128)(2,1)}, u32[]{:S(2)}) copy-start(bf16[16,2048]{1,0:T(8,128)(2,1)} %param.22) | copy-start | bytes 196612
  123.9 35.4 %copy-start.4 = (f32[2048]{0:T(1024)S(1)}, f32[2048]{0:T(1024)}, u32[]{:S(2)}) copy-start(f32[2048]{0:T(1024)} %param.21) | copy-start | bytes 24580
  123.9 23.1 %all-to-all-start = ((bf16[16,256,128]{1,2,0:T(8,128)(2,1)}), bf16[16,256,128]{1,2,0:T(8,128)(2,1)S(1)}, u32[]{:S(2)}, u32[]{:S(2)}) async-start(bf16[16,256,128]{1,2,0:T(8,128)(2,1)} %broadcast_in_dim.18), calls=%async_computation | async-start | bytes 2097152 | tf_op jit(solution)/shard_map/all_to_all | solution.py:29
  148.1 11.0 %all-to-all-start.1 = ((bf16[16,16,128]{2,1,0:T(8,128)(2,1)}), bf16[16,16,128]{2,1,0:T(8,128)(2,1)S(1)}, u32[]{:S(2)}, u32[]{:S(2)}) async-start(bf16[16,16,128]{2,1,0:T(8,128)(2,1)} %bitcast.12), calls=%async_computation.1 | async-start | bytes 131072 | tf_op jit(solution)/shard_map/all_to_all | solution.py:164
  152.6 92.9 %all-gather.5.cloned.1.call-start = ((), (), s32[]{:S(2)}) async-start(), calls=%async_computation.6 | async-start | bytes 4456448 | tf_op jit(solution)/shard_map/all_gather | solution.py:194
  159.3 86.2 %copy-start.6 = (bf16[1,2048,256]{2,1,0:T(8,128)(2,1)S(1)}, bf16[1,2048,256]{2,1,0:T(8,128)(2,1)}, u32[]{:S(2)}) copy-start(bf16[1,2048,256]{2,1,0:T(8,128)(2,1)} %param.25) | copy-start | bytes 3145732
  314.1 18.4 %copy-start.5 = (f32[16,2]{0,1:T(2,128)S(1)}, f32[16,2]{0,1:T(2,128)}, u32[]{:S(2)}) copy-start(f32[16,2]{0,1:T(2,128)} %param.24) | copy-start | bytes 388
  317.9 36.5 %all-to-all-start.4 = ((bf16[32,2,2048]{2,1,0:T(2,128)(2,1)}), bf16[32,2,2048]{2,1,0:T(2,128)(2,1)S(1)}, u32[]{:S(2)}, u32[]{:S(2)}) async-start(bf16[32,2,2048]{2,1,0:T(2,128)(2,1)} %all_to_all.39), calls=%async_computation.4 | async-start | bytes 524288 | tf_op jit(solution)/shard_map/all_to_all | solution.py:203
Sparse Core Ops, SparseCore 0:
  11.5 86.4 all-gather.2
  191.3 54.1 all-gather.4
where the time goes:
time: 364 us; the launch traced here: 363 us
  waiting for transfers between devices  185 us (51%)
  blocking collectives  85.5 us (23%)
  matrix products  27.4 us (8%)
  starting transfers between devices  25.5 us (7%)
  local copies, waits for them, and re-layouts  17.3 us (5%)
  between operations  13.7 us (4%)
  other arithmetic  9 us (2%)
    all_gather x1, waiting for transfers between devices, side_by_side(): result, at, done = (lax.all_gather(both, axis, axis=dim, tiled=True), 0, [])  86.4 us
    all_to_all x1, blocking collectives, sent_and_summed(): tiles = lax.all_to_all(split_up(value, dim, peers), axis, 0, 0, tiled=True)  55 us
    all_gather x1, waiting for transfers between devices, local(): piece = lax.all_gather(arrived, 'tp', axis=0, tiled=True)  54.4 us
    all_to_all x1, blocking collectives, local(): lax.all_to_all(send_rows, 'sp', split_axis=0, concat_axis=0, tiled=True)  30.5 us
    all_to_all x1, waiting for transfers between devices, local(): lax.all_to_all(expert_out, 'sp', split_axis=0, concat_axis=0, tiled=True)  21.9 us
    all_to_all x1, waiting for transfers between devices, copy_for_each(): return lax.all_to_all(copies, axis, split_axis=0, concat_axis=0, tiled=True)  15.7 us
    all_to_all x1, starting transfers between devices, local(): lax.all_to_all(expert_out, 'sp', split_axis=0, concat_axis=0, tiled=True)  14.3 us
    slice x3, local copies, waits for them, and re-layouts, side_by_side(): done.append(lax.slice_in_dim(result, at, at + a.shape[along], axis=along))  10.5 us
  transfers between devices with their start and end apart: 5, of which 5 were waited for; matrix products, arithmetic and copies ran while one was open for 0% of the time, Pallas kernels for 0%

commit v1 on v0

--- a/solution.py
+++ b/solution.py
@@ -191,7 +191,8 @@
     gate_weight = w_gate[0]
     up_weight = w_up[0]
     down_weight = w_down[0]
-    piece = lax.all_gather(arrived, "tp", axis=0, tiled=True)
+    copies_2 = jnp.concatenate([arrived] * lax.axis_size("tp"), axis=0)
+    piece = lax.all_to_all(copies_2, "tp", 0, 0, tiled=True)
     gate = jnp.dot(piece, gate_weight, preferred_element_type=jnp.float32)
     upper = jnp.dot(piece, up_weight, preferred_element_type=jnp.float32)
     hidden = (jax.nn.silu(gate) * upper).astype(jnp.bfloat16)

time: 364 us -> 356 us (0.978)
  waiting for transfers between devices: 185 us -> 131 us
  blocking collectives: 85.5 us -> 138 us
  starting transfers between devices: 25.5 us -> 18.2 us
    all_gather x1 -> x0, waiting for transfers between devices: 54.4 us -> none  [local(): piece = lax.all_gather(arrived, 'tp', axis=0, tiled=True)]
    all_to_all x0 -> x1, blocking collectives: none -> 52.8 us  [local(): piece = lax.all_to_all(copies_2, 'tp', 0, 0, tiled=True)]
    all_to_all x1, starting transfers between devices: 14.3 us -> 7.21 us  [local(): lax.all_to_all(expert_out, 'sp', split_axis=0, concat_axis=0, tiled=True)]
  transfers between devices with their start and end apart: 5 -> 4, of which waited for: 5 -> 4; matrix products, arithmetic and copies ran while one was open for 0% -> 0% of each run, Pallas kernels for 0% -> 0%
where the time goes in v1:
time: 356 us; the launch traced here: 355 us
  blocking collectives  138 us (39%)
  waiting for transfers between devices  131 us (37%)
  matrix products  26.3 us (7%)
  local copies, waits for them, and re-layouts  18.9 us (5%)
  starting transfers between devices  18.2 us (5%)
  between operations  13.8 us (4%)
  other arithmetic  9 us (3%)
    all_gather x1, waiting for transfers between devices, side_by_side(): result, at, done = (lax.all_gather(both, axis, axis=dim, tiled=True), 0, [])  86.4 us
    all_to_all x1, blocking collectives, sent_and_summed(): tiles = lax.all_to_all(split_up(value, dim, peers), axis, 0, 0, tiled=True)  54.3 us
    all_to_all x1, blocking collectives, local(): piece = lax.all_to_all(copies_2, 'tp', 0, 0, tiled=True)  52.8 us
    all_to_all x1, blocking collectives, local(): lax.all_to_all(send_rows, 'sp', split_axis=0, concat_axis=0, tiled=True)  30.5 us
    all_to_all x1, waiting for transfers between devices, local(): lax.all_to_all(expert_out, 'sp', split_axis=0, concat_axis=0, tiled=True)  21.9 us
    all_to_all x1, waiting for transfers between devices, copy_for_each(): return lax.all_to_all(copies, axis, split_axis=0, concat_axis=0, tiled=True)  15.7 us
    slice x3, local copies, waits for them, and re-layouts, side_by_side(): done.append(lax.slice_in_dim(result, at, at + a.shape[along], axis=along))  10.5 us
    dot_general x1, matrix products, local(): jnp.dot(hidden, down_weight, preferred_element_type=jnp.float32)  9.05 us
  transfers between devices with their start and end apart: 4, of which 4 were waited for; matrix products, arithmetic and copies ran while one was open for 0% of the time, Pallas kernels for 0%

profile of v1, /device:TPU:1, one launch (start us, length us, event | category | flops | bytes accessed | tf_op | source)
XLA Modules:
  0.0 354.5 jit_solution(7381393774509043917)
XLA Ops:
  6.6 1.0 constant_dynamic-slice_fusion
  7.5 0.1 copy.48
  7.7 0.9 copy.36
  8.8 0.7 fusion.25
  9.6 0.7 fusion.28
  10.3 0.3 fusion.55
  10.7 0.7 pad_maximum_fusion
  11.4 0.1 copy.39
  11.5 86.4 %all-gather.2.cloned.1.call-done = bf16[8192,256]{0,1:T(8,128)(2,1)} async-done(((bf16[256,256]{0,1:T(8,128)(2,1)}), bf16[8192,256]{0,1:T(8,128)(2,1)}) %all-gather.2.cloned.1.call-update) | async-done | bytes 4194320 | tf_op jit(solution)/shard_map/all_gather | solution.py:14
  97.9 3.9 %fusion.82 = (bf16[8192,128]{0,1:T(8,128)(2,1)S(1)}, bf16[8192,128]{0,1:T(8,128)(2,1)}) fusion(bf16[8192,256]{0,1:T(8,128)(2,1)} %all-gather.2.cloned.1.call-done), kind=kLoop, calls=%fused_computation.148 | loop fusion | bytes 8388608 | tf_op jit(solution)/shard_map/slice | solution.py:16
  101.8 4.1 %copy.35 = bf16[8192,128]{1,0:T(8,128)(2,1)} copy(bf16[8192,128]{0,1:T(8,128)(2,1)} %get-tuple-element.113) | data formatting | bytes 4194304 | tf_op jit(solution)/shard_map/slice | solution.py:16
  105.9 2.4 copy.37
  108.4 14.2 %while.15 = (s32[]{:T(128)}, f32[1,256]{1,0:T(1,128)S(1)}, f32[1,256]{1,0:T(1,128)S(1)}, f32[1,256,128]{2,1,0:T(8,128)S(1)}, bf16[4,2048,1,128]{3,1,2,0:T(8,128)...) while((s32[]{:T(128)}, f32[1,256]{1,0:T(1,128)S(1)}, ...), condition=%wide.region_5.6_spmd.clone, body=%wide.region_2.5_spmd.clone.sunk | while | flops 272729344 | bytes 7685225 | solution.py:105
  108.4 1.6 fusion.94
  110.0 0.4 convert_reduce_fusion.2
  110.4 1.6 fusion.97
  112.0 1.6 fusion.94
  113.5 0.4 convert_reduce_fusion.2
  113.9 1.6 fusion.97
  115.5 1.6 fusion.94
  117.1 0.4 convert_reduce_fusion.2
  117.5 1.6 fusion.97
  119.0 1.6 fusion.94
  120.6 0.4 convert_reduce_fusion.2
  121.0 1.6 fusion.97
  122.8 1.1 broadcast_in_dim.18
  123.9 6.5 %all-to-all-start = ((bf16[16,256,128]{1,2,0:T(8,128)(2,1)}), bf16[16,256,128]{1,2,0:T(8,128)(2,1)S(1)}, u32[]{:S(2)}, u32[]{:S(2)}) async-start(bf16[16,256,128]{1,2,0:T(8,128)(2,1)} %broadcast_in_dim.18), calls=%async_computation | async-start | bytes 2097152 | tf_op jit(solution)/shard_map/all_to_all | solution.py:29
  130.8 0.2 select_reduce_fusion
  131.2 15.7 %all-to-all-done = bf16[16,256,128]{1,2,0:T(8,128)(2,1)S(1)} async-done(((bf16[16,256,128]{1,2,0:T(8,128)(2,1)}), bf16[16,256,128]{1,2,0:T(8,128)(2,1)S(1)}, u32[]{:S(2)}, u32[]{:S(2)}) %all-to-all-start) | async-done | bytes 1048608 | tf_op jit(solution)/shard_map/all_to_all | solution.py:29
  146.9 2.2 convolution_convert_fusion.2
  149.1 4.5 %all-to-all-start.1 = ((bf16[16,16,128]{2,1,0:T(8,128)(2,1)}), bf16[16,16,128]{2,1,0:T(8,128)(2,1)S(1)}, u32[]{:S(2)}, u32[]{:S(2)}) async-start(bf16[16,16,128]{2,1,0:T(8,128)(2,1)} %bitcast.12), calls=%async_computation.1 | async-start | bytes 131072 | tf_op jit(solution)/shard_map/all_to_all | solution.py:164
  153.6 6.5 %all-to-all-done.1 = bf16[16,16,128]{2,1,0:T(8,128)(2,1)S(1)} async-done(((bf16[16,16,128]{2,1,0:T(8,128)(2,1)}), bf16[16,16,128]{2,1,0:T(8,128)(2,1)S(1)}, u32[]{:S(2)}, u32[]{:S(2)}) %all-to-all-start.1) | async-done | bytes 65568 | tf_op jit(solution)/shard_map/all_to_all | solution.py:164
  160.1 0.1 fusion.29
  160.2 0.3 convolution_convert_fusion.1
  160.5 0.2 all_to_all.43
  160.7 30.5 %all_to_all.59 = bf16[32,2,2048]{2,1,0:T(2,128)(2,1)S(1)} all-to-all(bf16[32,2,2048]{2,1,0:T(2,128)(2,1)S(1)} %all_to_all.43), channel_id=1, replica_groups=mesh['sp'=32,'tp'=16] {'sp'}, dimensions={0} | all-to-all | bytes 524288 | tf_op jit(solution)/shard_map/all_to_all | solution.py:190
  191.8 52.8 %all_to_all.60 = bf16[16,64,2048]{2,1,0:T(8,128)(2,1)S(1)} all-to-all(bf16[16,64,2048]{2,1,0:T(8,128)(2,1)S(1)} %bitcast.93), channel_id=1, replica_groups=mesh['sp'=32,'tp'=16] {'tp'}, dimensions={0} | all-to-all | bytes 8388608 | tf_op jit(solution)/shard_map/all_to_all | solution.py:195
  244.6 2.0 copy-done.1
  246.5 2.3 fusion.15
  248.9 9.1 %convolution_convert_fusion = bf16[1024,2048]{1,0:T(8,128)(2,1)} fusion(bf16[1024,2048]{1,0:T(8,128)(2,1)} %bitcast.95, bf16[1,256,2048]{2,1,0:T(8,128)(2,1)S(1)} %copy-done, bf16[1,2048,256]{2,1,0:T(8,128)(2,1)} %param.26, f32[1024,256]{1,0:T(8,128)} %fusion.15), kind=kOutput, calls=%fused_computation.20 | convolution fusion | flops 2151153664 | bytes 11534336 | tf_op jit(solution)/shard_map/dot_general | solution.py:200
  257.9 54.3 %all_to_all.61 = bf16[16,64,2048]{2,1,0:T(8,128)(2,1)} all-to-all(bf16[16,64,2048]{2,1,0:T(8,128)(2,1)} %bitcast.96), channel_id=1, replica_groups=mesh['sp'=32,'tp'=16] {'tp'}, dimensions={0} | all-to-all | bytes 8388608 | tf_op jit(solution)/shard_map/all_to_all | solution.py:43
  312.3 3.0 reduce_sum.90
  315.2 0.9 all_to_all.50
  316.1 7.2 %all-to-all-start.5 = ((bf16[32,2,2048]{2,1,0:T(2,128)(2,1)}), bf16[32,2,2048]{2,1,0:T(2,128)(2,1)S(1)}, u32[]{:S(2)}, u32[]{:S(2)}) async-start(bf16[32,2,2048]{2,1,0:T(2,128)(2,1)} %all_to_all.50), calls=%async_computation.5 | async-start | bytes 524288 | tf_op jit(solution)/shard_map/all_to_all | solution.py:204
  323.7 21.9 %all-to-all-done.5 = bf16[32,2,2048]{2,1,0:T(2,128)(2,1)S(1)} async-done(((bf16[32,2,2048]{2,1,0:T(2,128)(2,1)}), bf16[32,2,2048]{2,1,0:T(2,128)(2,1)S(1)}, u32[]{:S(2)}, u32[]{:S(2)}) %all-to-all-start.5) | async-done | bytes 262176 | tf_op jit(solution)/shard_map/all_to_all | solution.py:204
  345.7 0.7 gather_fusion
  346.5 0.6 multiply_reduce_fusion
  347.0 0.6 fusion.32
  (76 shorter events, 2.2 us)
Async XLA Ops:
  6.5 242.3 %copy-start = (bf16[1,256,2048]{2,1,0:T(8,128)(2,1)S(1)}, bf16[1,256,2048]{2,1,0:T(8,128)(2,1)}, u32[]{:S(2)}) copy-start(bf16[1,256,2048]{2,1,0:T(8,128)(2,1)} %param.27) | copy-start | bytes 3145732
  6.5 91.4 %all-gather.2.cloned.1.call-start = ((), (), s32[]{:S(2)}) async-start(), calls=%async_computation.6 | async-start | bytes 4325376 | tf_op jit(solution)/shard_map/all_gather | solution.py:14
  108.4 22.1 %copy-start.3 = (s32[16,2]{0,1:T(2,128)S(1)}, s32[16,2]{0,1:T(2,128)}, u32[]{:S(2)}) copy-start(s32[16,2]{0,1:T(2,128)} %param.23) | copy-start | bytes 388
  122.6 37.5 %copy-start.2 = (bf16[16,2048]{1,0:T(8,128)(2,1)S(1)}, bf16[16,2048]{1,0:T(8,128)(2,1)}, u32[]{:S(2)}) copy-start(bf16[16,2048]{1,0:T(8,128)(2,1)} %param.22) | copy-start | bytes 196612
  122.6 37.6 %copy-start.4 = (f32[2048]{0:T(1024)S(1)}, f32[2048]{0:T(1024)}, u32[]{:S(2)}) copy-start(f32[2048]{0:T(1024)} %param.21) | copy-start | bytes 24580
  123.9 23.0 %all-to-all-start = ((bf16[16,256,128]{1,2,0:T(8,128)(2,1)}), bf16[16,256,128]{1,2,0:T(8,128)(2,1)S(1)}, u32[]{:S(2)}, u32[]{:S(2)}) async-start(bf16[16,256,128]{1,2,0:T(8,128)(2,1)} %broadcast_in_dim.18), calls=%async_computation | async-start | bytes 2097152 | tf_op jit(solution)/shard_map/all_to_all | solution.py:29
  149.1 11.0 %all-to-all-start.1 = ((bf16[16,16,128]{2,1,0:T(8,128)(2,1)}), bf16[16,16,128]{2,1,0:T(8,128)(2,1)S(1)}, u32[]{:S(2)}, u32[]{:S(2)}) async-start(bf16[16,16,128]{2,1,0:T(8,128)(2,1)} %bitcast.12), calls=%async_computation.1 | async-start | bytes 131072 | tf_op jit(solution)/shard_map/all_to_all | solution.py:164
  191.8 54.8 %copy-start.6 = (bf16[1,2048,256]{2,1,0:T(8,128)(2,1)S(1)}, bf16[1,2048,256]{2,1,0:T(8,128)(2,1)}, u32[]{:S(2)}) copy-start(bf16[1,2048,256]{2,1,0:T(8,128)(2,1)} %param.25) | copy-start | bytes 3145732
  244.6 2.0 copy-start.1
  312.3 11.4 %copy-start.5 = (f32[16,2]{0,1:T(2,128)S(1)}, f32[16,2]{0,1:T(2,128)}, u32[]{:S(2)}) copy-start(f32[16,2]{0,1:T(2,128)} %param.24) | copy-start | bytes 388
  316.1 29.5 %all-to-all-start.5 = ((bf16[32,2,2048]{2,1,0:T(2,128)(2,1)}), bf16[32,2,2048]{2,1,0:T(2,128)(2,1)S(1)}, u32[]{:S(2)}, u32[]{:S(2)}) async-start(bf16[32,2,2048]{2,1,0:T(2,128)(2,1)} %all_to_all.50), calls=%async_computation.5 | async-start | bytes 524288 | tf_op jit(solution)/shard_map/all_to_all | solution.py:204
Sparse Core Ops, SparseCore 0:
  11.5 86.4 all-gather.1
